TPU v7x, 256 devices: a 4x2x16 block of a 4x16x16 slice. The times are simulated.
256 devices in a mesh: grp: 2 (over y), fs: 32 (over z, core), tp: 4 (over x).
Axes of the slice: x: 4, y: 2, z: 16, core: 2. Of those that a mesh axis runs over, the one named last changes fastest.
The devices are a block of a 4x16x16 slice.
Arguments:
- prompt: bfloat16 [8, 1024, 2048], P(('grp', 'tp')), parts along dimension 0, may hold values from -6 to 6
- gate_first: float32 [2048, 5632], P('fs', 'tp'), may hold values from -0.125 to 0.125
- up_first: float32 [2048, 5632], P('fs', 'tp'), may hold values from -0.125 to 0.125
- down_first: float32 [5632, 2048], P('fs', 'tp'), may hold values from -0.3125 to 0.3125
- norm_gain: float32 [2048], replicated, may hold values from 0.1 to 1.9
- gate_second: float32 [2048, 5632], P('fs', 'tp'), may hold values from -0.125 to 0.125
- up_second: float32 [2048, 5632], P('fs', 'tp'), may hold values from -0.125 to 0.125
- down_second: float32 [5632, 2048], P('fs', 'tp'), may hold values from -0.3125 to 0.3125
Outputs:
- result: bfloat16 [8, 1024, 2048], P(('grp', 'tp'), 'fs'), parts along dimension 0
- gate_one: bfloat16 [4096, 5632], P('grp', 'fs'), parts along dimension 0
- up_one: bfloat16 [4096, 5632], P('grp', 'fs'), parts along dimension 0
- down_one: bfloat16 [5632, 4096], P('fs', 'grp'), parts along dimension 1
- gate_two: bfloat16 [4096, 5632], P('grp', 'fs'), parts along dimension 0
- up_two: bfloat16 [4096, 5632], P('grp', 'fs'), parts along dimension 0
- down_two: bfloat16 [5632, 4096], P('fs', 'grp'), parts along dimension 1
There are 2 independent parts, one for each index of `grp`. A program takes and returns all parts, laid end to end along the dimension named above; an argument that names none is the same for every part. Nothing has to cross between parts.
All inputs are finite; a program needn't handle non-finite values.
Results may differ from a plain program's by a relative error of at most 0.029.
Values may be sent and summed in bfloat16 or wider, within the bound.
A program may use at most 64 MiB of HBM per device.

v0:
```python
import jax
import jax.numpy as jnp
from jax import lax
from jax.sharding import Mesh
from jax.sharding import PartitionSpec as P

FS = ("fs_0", "fs_1")
norm_eps = 1e-05
deep_alpha = 2.0**0.25
half_step = 0.5


def reduced_to_own(pieces, axes, sequence):
    inside = pieces.shape[1:]
    pieces = pieces.reshape(*(lax.axis_size(a) for a in axes), *inside)
    pieces = jnp.moveaxis(pieces, sequence, range(len(axes))).reshape(-1, *inside)
    for k in sequence:
        pieces = lax.psum_scatter(pieces, axes[k], scatter_dimension=0, tiled=True)
    return pieces[0]


def cut_along(value, dim, size):
    before, after = (value.shape[:dim], value.shape[dim + 1 :])
    return jnp.moveaxis(value.reshape(*before, size, -1, *after), dim, 0)


def scatter_axes(value, axes, sequence, dim):
    size = lax.axis_size(axes)
    return reduced_to_own(cut_along(value, dim, size), axes, sequence)


def plain_norm(values):
    row_mean = jnp.mean(values, axis=-1, keepdims=True)
    centred = values - row_mean
    variance = jnp.mean(centred * centred, axis=-1, keepdims=True)
    return centred * lax.rsqrt(variance + norm_eps)


def gated_hidden(inputs, gate_proj, up_proj):
    gate_act = jnp.dot(inputs, gate_proj, preferred_element_type=jnp.float32)
    up_act = jnp.dot(inputs, up_proj, preferred_element_type=jnp.float32)
    return (jax.nn.silu(gate_act) * up_act).astype(jnp.bfloat16)


def relay_weights(gate_proj, up_proj, down_proj):
    gate_rows, up_rows, down_mine = (
        lax.all_gather(gate_proj, "tp", axis=1, tiled=True),
        lax.all_gather(up_proj, "tp", axis=1, tiled=True),
        lax.all_gather(down_proj, "tp", axis=1, tiled=True),
    )
    gate_mine, up_mine = (
        lax.all_to_all(gate_rows, FS, split_axis=1, concat_axis=0, tiled=True),
        lax.all_to_all(up_rows, FS, split_axis=1, concat_axis=0, tiled=True),
    )
    return (gate_mine, up_mine, down_mine)


def row_terms(hidden, down_proj):
    return jnp.dot(hidden, down_proj, preferred_element_type=jnp.float32)


def body(prompt, gate_first, up_first, down_first, norm_gain, gate_second, up_second, down_second):
    fs_index = lax.axis_index(FS)
    row_block = gate_first.shape[0]
    gain_rows = lax.dynamic_slice_in_dim(norm_gain, fs_index * row_block, row_block, 0)
    gate_one, up_one, down_one = relay_weights(
        gate_first.astype(jnp.bfloat16),
        up_first.astype(jnp.bfloat16),
        down_first.astype(jnp.bfloat16),
    )
    gate_two, up_two, down_two = relay_weights(
        (gain_rows[:, None] * gate_second).astype(jnp.bfloat16),
        (gain_rows[:, None] * up_second).astype(jnp.bfloat16),
        down_second.astype(jnp.bfloat16),
    )
    tokens = prompt.reshape(-1, prompt.shape[-1])
    own_count = tokens.shape[0] // lax.axis_size(FS)
    own_first = fs_index * own_count
    hidden_one = gated_hidden(tokens, gate_one, up_one)
    own_tokens = lax.dynamic_slice_in_dim(tokens, own_first, own_count, 0)
    ffn_one = scatter_axes(
        row_terms(hidden_one, down_one).astype(jnp.bfloat16), FS, (1, 0), 0
    ).astype(jnp.float32)
    normed_own = plain_norm(
        deep_alpha * own_tokens.astype(jnp.float32) + half_step * ffn_one
    ).astype(jnp.bfloat16)
    hidden_two = gated_hidden(lax.all_gather(normed_own, FS, axis=0, tiled=True), gate_two, up_two)
    ffn_two = scatter_axes(
        row_terms(hidden_two, down_two).astype(jnp.bfloat16), FS, (1, 0), 0
    ).astype(jnp.float32)
    residual_two = deep_alpha * norm_gain * normed_own.astype(jnp.float32)
    result = plain_norm(residual_two + half_step * ffn_two).astype(jnp.bfloat16)
    return (
        result.reshape(1, result.shape[0], result.shape[-1]),
        gate_one,
        up_one,
        down_one,
        gate_two,
        up_two,
        down_two,
    )


def solution(mesh):
    torus = Mesh(
        mesh.devices.reshape(mesh.shape["grp"], 16, 2, mesh.shape["tp"]),
        ("grp", "fs_0", "fs_1", "tp"),
    )
    placed = (
        P(("grp", "tp"), None, None),
        P(FS, "tp"),
        P(FS, "tp"),
        P(FS, "tp"),
        P(),
        P(FS, "tp"),
        P(FS, "tp"),
        P(FS, "tp"),
    )
    return jax.shard_map(
        body,
        mesh=torus,
        in_specs=placed,
        out_specs=(
            P(("grp", "tp"), FS, None),
            P("grp", FS),
            P("grp", FS),
            P(FS, "grp"),
            P("grp", FS),
            P("grp", FS),
            P(FS, "grp"),
        ),
        check_vma=False,
    )
```

profile of v0, /device:TPU:34, one launch (start us, length us, event | category | flops | bytes accessed | tf_op | source)
XLA Modules:
  0.0 540.0 jit_solution(11706451847986128299)
XLA Ops:
  8.2 29.5 %all_gather.21 = bf16[64,5632]{1,0:T(8,128)(2,1)S(1)} all-gather(bf16[64,1408]{1,0:T(8,128)(2,1)S(1)} %convert_element_type.62), channel_id=1, replica_groups=mesh['grp'=2,'fs_0'=16,'fs_1'=2,'tp'=4] {'tp'}, dimensions={1}, use_global_device_ids=true | all-gather | bytes 901120 | tf_op jit(solution)/shard_map/all_gather | solution.py:47
  37.8 2.0 all_to_all.56
  41.4 9.7 %all-to-all-start = ((bf16[64,32,176]{2,0,1:T(8,128)(2,1)}), bf16[64,32,176]{2,0,1:T(8,128)(2,1)S(1)}, u32[]{:S(2)}, u32[]{:S(2)}) async-start(bf16[64,32,176]{2,0,1:T(8,128)(2,1)} %copy.21), calls=%async_computation | async-start | bytes 2097152 | tf_op jit(solution)/shard_map/all_to_all | solution.py:52
  51.2 14.4 %all_gather.22 = bf16[64,5632]{1,0:T(8,128)(2,1)S(1)} all-gather(bf16[64,1408]{1,0:T(8,128)(2,1)S(1)} %convert_element_type.63), channel_id=1, replica_groups=mesh['grp'=2,'fs_0'=16,'fs_1'=2,'tp'=4] {'tp'}, dimensions={1}, use_global_device_ids=true | all-gather | bytes 901120 | tf_op jit(solution)/shard_map/all_gather | solution.py:48
  65.5 2.0 all_to_all.60
  69.1 37.3 %all-to-all-done = bf16[64,32,176]{2,0,1:T(8,128)(2,1)S(1)} async-done(((bf16[64,32,176]{2,0,1:T(8,128)(2,1)}), bf16[64,32,176]{2,0,1:T(8,128)(2,1)S(1)}, u32[]{:S(2)}, u32[]{:S(2)}) %all-to-all-start) | async-done | bytes 720928 | tf_op jit(solution)/shard_map/all_to_all | solution.py:52
  106.4 4.8 all-to-all-start.1
  111.4 14.2 %all_gather.23 = bf16[176,2048]{1,0:T(8,128)(2,1)S(1)} all-gather(bf16[176,512]{1,0:T(8,128)(2,1)S(1)} %convert_element_type.65), channel_id=1, replica_groups=mesh['grp'=2,'fs_0'=16,'fs_1'=2,'tp'=4] {'tp'}, dimensions={1}, use_global_device_ids=true | all-gather | bytes 901120 | tf_op jit(solution)/shard_map/all_gather | solution.py:49
  125.6 4.0 fusion.2
  129.6 37.3 %all-to-all-done.1 = bf16[64,32,176]{2,0,1:T(8,128)(2,1)S(1)} async-done(((bf16[64,32,176]{2,0,1:T(8,128)(2,1)}), bf16[64,32,176]{2,0,1:T(8,128)(2,1)S(1)}, u32[]{:S(2)}, u32[]{:S(2)}) %all-to-all-start.1) | async-done | bytes 720928 | tf_op jit(solution)/shard_map/all_to_all | solution.py:53
  167.0 7.0 %convolution_convert_fusion.1 = bf16[1024,2048]{1,0:T(8,128)(2,1)} fusion(bf16[176,2048]{1,0:T(8,128)(2,1)S(1)} %all_gather.23, bf16[2048,176]{1,0:T(8,128)(2,1)S(1)} %bitcast.57, bf16[1,1024,2048]{2,1,0:T(8,128)(2,1)} %param.8, f32[1024,176]{0,1:T(8,128)S(1)} %fusion.2), kind=kOutput, calls=%fused_computation.5 | convolution fusion | flops 1479573504 | bytes 10551296 | tf_op jit(solution)/shard_map/dot_general | solution.py:59
  173.9 4.7 copy.23
  178.8 12.5 %reduce-scatter.5.cloned.1.call-done = bf16[16,32,2048]{2,1,0:T(8,128)(2,1)} async-done(((bf16[32,32,2048]{2,1,0:T(8,128)(2,1)}), bf16[16,32,2048]{2,1,0:T(8,128)(2,1)}) %reduce-scatter.5.cloned.1.call-update) | async-done | bytes 2097168 | tf_op jit(solution)/shard_map/reduce_scatter | solution.py:18
  191.4 75.9 %reduce-scatter.7.cloned.1.call-done = bf16[1,32,2048]{2,1,0:T(8,128)(2,1)} async-done(((bf16[16,32,2048]{2,1,0:T(8,128)(2,1)}), bf16[1,32,2048]{2,1,0:T(8,128)(2,1)}) %reduce-scatter.7.cloned.1.call-update) | async-done | bytes 131088 | tf_op jit(solution)/shard_map/reduce_scatter | solution.py:18
  269.7 1.7 multiply_convert_fusion.3
  271.7 14.1 %all_gather.25 = bf16[64,5632]{1,0:T(8,128)(2,1)} all-gather(bf16[64,1408]{1,0:T(8,128)(2,1)S(1)} %get-tuple-element.14), channel_id=1, replica_groups=mesh['grp'=2,'fs_0'=16,'fs_1'=2,'tp'=4] {'tp'}, dimensions={1}, use_global_device_ids=true | all-gather | bytes 901120 | tf_op jit(solution)/shard_map/all_gather | solution.py:47
  285.8 3.0 all_to_all.64
  290.4 9.7 %all-to-all-start.2 = ((bf16[64,32,176]{2,0,1:T(8,128)(2,1)}), bf16[64,32,176]{2,0,1:T(8,128)(2,1)S(1)}, u32[]{:S(2)}, u32[]{:S(2)}) async-start(bf16[64,32,176]{2,0,1:T(8,128)(2,1)} %copy.24), calls=%async_computation.4 | async-start | bytes 2097152 | tf_op jit(solution)/shard_map/all_to_all | solution.py:52
  300.1 14.3 %all_gather.26 = bf16[64,5632]{1,0:T(8,128)(2,1)} all-gather(bf16[64,1408]{1,0:T(8,128)(2,1)S(1)} %get-tuple-element.15), channel_id=1, replica_groups=mesh['grp'=2,'fs_0'=16,'fs_1'=2,'tp'=4] {'tp'}, dimensions={1}, use_global_device_ids=true | all-gather | bytes 901120 | tf_op jit(solution)/shard_map/all_gather | solution.py:48
  314.4 3.8 all_to_all.68
  318.2 2.8 copy.25
  321.0 44.7 %all-to-all-done.2 = bf16[64,32,176]{2,0,1:T(8,128)(2,1)S(1)} async-done(((bf16[64,32,176]{2,0,1:T(8,128)(2,1)}), bf16[64,32,176]{2,0,1:T(8,128)(2,1)S(1)}, u32[]{:S(2)}, u32[]{:S(2)}) %all-to-all-start.2) | async-done | bytes 720928 | tf_op jit(solution)/shard_map/all_to_all | solution.py:52
  365.7 5.7 %all-to-all-start.3 = ((bf16[64,32,176]{2,0,1:T(8,128)(2,1)}), bf16[64,32,176]{2,0,1:T(8,128)(2,1)}, u32[]{:S(2)}, u32[]{:S(2)}) async-start(bf16[64,32,176]{2,0,1:T(8,128)(2,1)} %copy.25), calls=%async_computation.5 | async-start | bytes 2097152 | tf_op jit(solution)/shard_map/all_to_all | solution.py:53
  371.5 14.5 %all_gather.27 = bf16[176,2048]{1,0:T(8,128)(2,1)} all-gather(bf16[176,512]{1,0:T(8,128)(2,1)S(1)} %convert_element_type.74), channel_id=1, replica_groups=mesh['grp'=2,'fs_0'=16,'fs_1'=2,'tp'=4] {'tp'}, dimensions={1}, use_global_device_ids=true | all-gather | bytes 901120 | tf_op jit(solution)/shard_map/all_gather | solution.py:49
  386.0 4.6 fusion.29
  390.6 36.6 %all-to-all-done.3 = bf16[64,32,176]{2,0,1:T(8,128)(2,1)} async-done(((bf16[64,32,176]{2,0,1:T(8,128)(2,1)}), bf16[64,32,176]{2,0,1:T(8,128)(2,1)}, u32[]{:S(2)}, u32[]{:S(2)}) %all-to-all-start.3) | async-done | bytes 720928 | tf_op jit(solution)/shard_map/all_to_all | solution.py:53
  427.2 7.7 %convolution_convert_fusion = bf16[1024,2048]{1,0:T(8,128)(2,1)} fusion(bf16[176,2048]{1,0:T(8,128)(2,1)} %all_gather.27, bf16[1024,2048]{1,0:T(8,128)(2,1)} %all-gather.2.cloned.1.call-done, bf16[2048,176]{1,0:T(8,128)(2,1)} %bitcast.12, f32[1024,176]{0,1:T(8,128)} %fusion.29), kind=kOutput, calls=%fused_computation.4 | convolution fusion | flops 1479573504 | bytes 10551296 | tf_op jit(solution)/shard_map/dot_general | solution.py:59
  434.9 4.7 copy.26
  439.7 11.8 %reduce-scatter.9.cloned.1.call-done = bf16[16,32,2048]{2,1,0:T(8,128)(2,1)} async-done(((bf16[32,32,2048]{2,1,0:T(8,128)(2,1)}), bf16[16,32,2048]{2,1,0:T(8,128)(2,1)}) %reduce-scatter.9.cloned.1.call-update) | async-done | bytes 2097168 | tf_op jit(solution)/shard_map/reduce_scatter | solution.py:18
  452.9 2.3 copy.30
  457.6 70.1 %reduce-scatter.11.cloned.1.call-done = bf16[1,32,2048]{2,1,0:T(8,128)(2,1)} async-done(((bf16[16,32,2048]{2,1,0:T(8,128)(2,1)}), bf16[1,32,2048]{2,1,0:T(8,128)(2,1)}) %reduce-scatter.11.cloned.1.call-update) | async-done | bytes 131088 | tf_op jit(solution)/shard_map/reduce_scatter | solution.py:18
  529.9 1.9 multiply_convert_fusion.2
  (52 shorter events, 16.6 us)
Async XLA Ops:
  7.2 43.9 %copy-start.3 = (f32[64,1408]{1,0:T(8,128)S(1)}, f32[64,1408]{1,0:T(8,128)}, u32[]{:S(2)}) copy-start(f32[64,1408]{1,0:T(8,128)} %param.10) | copy-start | bytes 1081348
  41.4 65.0 %all-to-all-start = ((bf16[64,32,176]{2,0,1:T(8,128)(2,1)}), bf16[64,32,176]{2,0,1:T(8,128)(2,1)S(1)}, u32[]{:S(2)}, u32[]{:S(2)}) async-start(bf16[64,32,176]{2,0,1:T(8,128)(2,1)} %copy.21), calls=%async_computation | async-start | bytes 2097152 | tf_op jit(solution)/shard_map/all_to_all | solution.py:52
  51.1 60.2 %copy-start.4 = (f32[176,512]{1,0:T(8,128)S(1)}, f32[176,512]{1,0:T(8,128)}, u32[]{:S(2)}) copy-start(f32[176,512]{1,0:T(8,128)} %param.11) | copy-start | bytes 1081348
  106.4 60.6 %all-to-all-start.1 = ((bf16[64,32,176]{2,0,1:T(8,128)(2,1)}), bf16[64,32,176]{2,0,1:T(8,128)(2,1)S(1)}, u32[]{:S(2)}, u32[]{:S(2)}) async-start(bf16[64,32,176]{2,0,1:T(8,128)(2,1)} %copy.22), calls=%async_computation.1 | async-start | bytes 2097152 | tf_op jit(solution)/shard_map/all_to_all | solution.py:53
  111.3 80.0 %reduce-scatter.5.cloned.1.call-start = ((), (), s32[]{:S(2)}) async-start(), calls=%async_computation.8 | async-start | bytes 6291456 | tf_op jit(solution)/shard_map/reduce_scatter | solution.py:18
  125.6 41.4 %copy-start = (bf16[176,2048]{1,0:T(8,128)(2,1)}, bf16[176,2048]{1,0:T(8,128)(2,1)S(1)}, u32[]{:S(2)}) copy-start(bf16[176,2048]{1,0:T(8,128)(2,1)S(1)} %all_gather.23) | copy-start | bytes 2162692
  178.7 92.8 %copy-start.8 = (f32[2048]{0:T(1024)S(1)}, f32[2048]{0:T(1024)}, u32[]{:S(2)}) copy-start(f32[2048]{0:T(1024)} %param.12) | copy-start | bytes 24580
  178.7 92.9 %copy-start.6 = (f32[64,1408]{1,0:T(8,128)S(1)}, f32[64,1408]{1,0:T(8,128)}, u32[]{:S(2)}) copy-start(f32[64,1408]{1,0:T(8,128)} %param.13) | copy-start | bytes 1081348
  178.7 92.9 %copy-start.7 = (f32[64,1408]{1,0:T(8,128)S(1)}, f32[64,1408]{1,0:T(8,128)}, u32[]{:S(2)}) copy-start(f32[64,1408]{1,0:T(8,128)} %param.14) | copy-start | bytes 1081348
  178.7 88.6 %reduce-scatter.7.cloned.1.call-start = ((), (), s32[]{:S(2)}) async-start(), calls=%async_computation.9 | async-start | bytes 2228224 | tf_op jit(solution)/shard_map/reduce_scatter | solution.py:18
  191.3 194.7 %all-gather.2.cloned.1.call-start = ((), (), s32[]{:S(2)}) async-start(), calls=%async_computation.10 | async-start | bytes 4325376 | tf_op jit(solution)/shard_map/all_gather | solution.py:87
  290.4 75.3 %all-to-all-start.2 = ((bf16[64,32,176]{2,0,1:T(8,128)(2,1)}), bf16[64,32,176]{2,0,1:T(8,128)(2,1)S(1)}, u32[]{:S(2)}, u32[]{:S(2)}) async-start(bf16[64,32,176]{2,0,1:T(8,128)(2,1)} %copy.24), calls=%async_computation.4 | async-start | bytes 2097152 | tf_op jit(solution)/shard_map/all_to_all | solution.py:52
  314.4 57.1 %copy-start.5 = (f32[176,512]{1,0:T(8,128)S(1)}, f32[176,512]{1,0:T(8,128)}, u32[]{:S(2)}) copy-start(f32[176,512]{1,0:T(8,128)} %param.15) | copy-start | bytes 1081348
  365.7 61.5 %all-to-all-start.3 = ((bf16[64,32,176]{2,0,1:T(8,128)(2,1)}), bf16[64,32,176]{2,0,1:T(8,128)(2,1)}, u32[]{:S(2)}, u32[]{:S(2)}) async-start(bf16[64,32,176]{2,0,1:T(8,128)(2,1)} %copy.25), calls=%async_computation.5 | async-start | bytes 2097152 | tf_op jit(solution)/shard_map/all_to_all | solution.py:53
  371.4 80.1 %reduce-scatter.9.cloned.1.call-start = ((), (), s32[]{:S(2)}) async-start(), calls=%async_computation.11 | async-start | bytes 6291456 | tf_op jit(solution)/shard_map/reduce_scatter | solution.py:18
  439.7 87.9 %reduce-scatter.11.cloned.1.call-start = ((), (), s32[]{:S(2)}) async-start(), calls=%async_computation.12 | async-start | bytes 2228224 | tf_op jit(solution)/shard_map/reduce_scatter | solution.py:18
  452.9 78.9 %copy-start.1 = (bf16[176,2048]{1,0:T(8,128)(2,1)S(1)}, bf16[176,2048]{1,0:T(8,128)(2,1)}, u32[]{:S(2)}) copy-start(bf16[176,2048]{1,0:T(8,128)(2,1)} %copy-done) | copy-start | bytes 2162692
  452.9 79.8 %copy-start.2 = (bf16[176,2048]{1,0:T(8,128)(2,1)S(1)}, bf16[176,2048]{1,0:T(8,128)(2,1)}, u32[]{:S(2)}) copy-start(bf16[176,2048]{1,0:T(8,128)(2,1)} %all_gather.27) | copy-start | bytes 2162692
Sparse Core Ops, SparseCore 0:
  178.9 12.3 reduce-scatter.4
  193.8 73.4 reduce-scatter.6
  271.6 98.2 all-gather.1
  439.8 11.7 reduce-scatter.8
  454.0 73.5 reduce-scatter.10
where the time goes:
time: 541 us; the launch traced here: 540 us
  waiting for transfers between devices  326 us (60%)
  blocking collectives  101 us (19%)
  local copies, waits for them, and re-layouts  35.6 us (7%)
  starting transfers between devices  30.2 us (6%)
  matrix products  23.2 us (4%)
  between operations  14 us (3%)
  other arithmetic  9.45 us (2%)
    reduce_scatter x4, waiting for transfers between devices, reduced_to_own(): pieces = lax.psum_scatter(pieces, axes[k], scatter_dimension=0, tiled=True)  170 us
    all_to_all x2, waiting for transfers between devices, relay_weights(): lax.all_to_all(gate_rows, FS, split_axis=1, concat_axis=0, tiled=True)  82 us
    all_to_all x2, waiting for transfers between devices, relay_weights(): lax.all_to_all(up_rows, FS, split_axis=1, concat_axis=0, tiled=True)  73.9 us
    all_gather x2, blocking collectives, relay_weights(): lax.all_gather(gate_proj, 'tp', axis=1, tiled=True)  43.7 us
    all_gather x2, blocking collectives, relay_weights(): lax.all_gather(down_proj, 'tp', axis=1, tiled=True)  28.7 us
    all_gather x2, blocking collectives, relay_weights(): lax.all_gather(up_proj, 'tp', axis=1, tiled=True)  28.6 us
    all_to_all x2, starting transfers between devices, relay_weights(): lax.all_to_all(gate_rows, FS, split_axis=1, concat_axis=0, tiled=True)  19.4 us
    dot_general x2, matrix products, row_terms(): return jnp.dot(hidden, down_proj, preferred_element_type=jnp.float32)  14.6 us
  transfers between devices with their start and end apart: 9, of which 8 were waited for; matrix products, arithmetic and copies ran while one was open for 4% of the time, Pallas kernels for 0%

commit v1 on v0

--- a/solution.py
+++ b/solution.py
@@ -44,7 +44,7 @@
 
 def relay_weights(gate_proj, up_proj, down_proj):
     gate_rows, up_rows, down_mine = (
-        lax.all_gather(gate_proj, "tp", axis=1, tiled=True),
+        jnp.concatenate(lax.all_gather(gate_proj, "tp"), axis=1),
         lax.all_gather(up_proj, "tp", axis=1, tiled=True),
         lax.all_gather(down_proj, "tp", axis=1, tiled=True),
     )

time: 541 us -> 541 us (level)
  no operation moved by 1% of the time
where the time goes in v1:
time: 541 us; the launch traced here: 540 us
  waiting for transfers between devices  326 us (60%)
  blocking collectives  100 us (18%)
  local copies, waits for them, and re-layouts  36.8 us (7%)
  starting transfers between devices  30.2 us (6%)
  matrix products  23.2 us (4%)
  between operations  14 us (3%)
  other arithmetic  9.4 us (2%)
    reduce_scatter x4, waiting for transfers between devices, reduced_to_own(): pieces = lax.psum_scatter(pieces, axes[k], scatter_dimension=0, tiled=True)  170 us
    all_to_all x2, waiting for transfers between devices, relay_weights(): lax.all_to_all(gate_rows, FS, split_axis=1, concat_axis=0, tiled=True)  81.6 us
    all_to_all x2, waiting for transfers between devices, relay_weights(): lax.all_to_all(up_rows, FS, split_axis=1, concat_axis=0, tiled=True)  74.2 us
    all_gather x2, blocking collectives, relay_weights(): lax.all_gather(gate_proj, 'tp')  42.8 us
    all_gather x2, blocking collectives, relay_weights(): lax.all_gather(up_proj, 'tp', axis=1, tiled=True)  28.8 us
    all_gather x2, blocking collectives, relay_weights(): lax.all_gather(down_proj, 'tp', axis=1, tiled=True)  28.4 us
    all_to_all x2, starting transfers between devices, relay_weights(): lax.all_to_all(gate_rows, FS, split_axis=1, concat_axis=0, tiled=True)  19.4 us
    dot_general x2, matrix products, row_terms(): return jnp.dot(hidden, down_proj, preferred_element_type=jnp.float32)  14.6 us
  transfers between devices with their start and end apart: 9, of which 8 were waited for; matrix products, arithmetic and copies ran while one was open for 4% of the time, Pallas kernels for 0%

profile of v1, /device:TPU:34, one launch (start us, length us, event | category | flops | bytes accessed | tf_op | source)
XLA Modules:
  0.0 540.1 jit_solution(3214939865761774351)
XLA Ops:
  8.2 29.6 %all-gather = bf16[256,1408]{1,0:T(8,128)(2,1)S(1)} all-gather(bf16[64,1408]{1,0:T(8,128)(2,1)S(1)} %convert_element_type.62), channel_id=2, replica_groups=mesh['grp'=2,'fs_0'=16,'fs_1'=2,'tp'=4] {'tp'}, dimensions={0}, use_global_device_ids=true | all-gather | bytes 901120 | tf_op jit(solution)/shard_map/all_gather | solution.py:47
  39.9 1.6 copy.32
  41.5 9.6 %all-to-all-start = ((bf16[64,32,176]{2,0,1:T(8,128)(2,1)}), bf16[64,32,176]{2,0,1:T(8,128)(2,1)S(1)}, u32[]{:S(2)}, u32[]{:S(2)}) async-start(bf16[64,32,176]{2,0,1:T(8,128)(2,1)} %copy.32), calls=%async_computation | async-start | bytes 2097152 | tf_op jit(solution)/shard_map/all_to_all | solution.py:52
  51.2 14.4 %all_gather.29 = bf16[64,5632]{1,0:T(8,128)(2,1)S(1)} all-gather(bf16[64,1408]{1,0:T(8,128)(2,1)S(1)} %convert_element_type.63), channel_id=1, replica_groups=mesh['grp'=2,'fs_0'=16,'fs_1'=2,'tp'=4] {'tp'}, dimensions={1}, use_global_device_ids=true | all-gather | bytes 901120 | tf_op jit(solution)/shard_map/all_gather | solution.py:48
  65.6 2.0 all_to_all.60
  69.2 37.2 %all-to-all-done = bf16[64,32,176]{2,0,1:T(8,128)(2,1)S(1)} async-done(((bf16[64,32,176]{2,0,1:T(8,128)(2,1)}), bf16[64,32,176]{2,0,1:T(8,128)(2,1)S(1)}, u32[]{:S(2)}, u32[]{:S(2)}) %all-to-all-start) | async-done | bytes 720928 | tf_op jit(solution)/shard_map/all_to_all | solution.py:52
  106.4 4.8 all-to-all-start.1
  111.4 14.3 %all_gather.30 = bf16[176,2048]{1,0:T(8,128)(2,1)S(1)} all-gather(bf16[176,512]{1,0:T(8,128)(2,1)S(1)} %convert_element_type.65), channel_id=1, replica_groups=mesh['grp'=2,'fs_0'=16,'fs_1'=2,'tp'=4] {'tp'}, dimensions={1}, use_global_device_ids=true | all-gather | bytes 901120 | tf_op jit(solution)/shard_map/all_gather | solution.py:49
  125.7 4.0 fusion.2
  129.7 37.3 %all-to-all-done.1 = bf16[64,32,176]{2,0,1:T(8,128)(2,1)S(1)} async-done(((bf16[64,32,176]{2,0,1:T(8,128)(2,1)}), bf16[64,32,176]{2,0,1:T(8,128)(2,1)S(1)}, u32[]{:S(2)}, u32[]{:S(2)}) %all-to-all-start.1) | async-done | bytes 720928 | tf_op jit(solution)/shard_map/all_to_all | solution.py:53
  167.0 7.0 %convolution_convert_fusion.1 = bf16[1024,2048]{1,0:T(8,128)(2,1)} fusion(bf16[176,2048]{1,0:T(8,128)(2,1)S(1)} %all_gather.30, bf16[2048,176]{1,0:T(8,128)(2,1)S(1)} %bitcast.65, bf16[1,1024,2048]{2,1,0:T(8,128)(2,1)} %param.8, f32[1024,176]{0,1:T(8,128)S(1)} %fusion.2), kind=kOutput, calls=%fused_computation.5 | convolution fusion | flops 1479573504 | bytes 10551296 | tf_op jit(solution)/shard_map/dot_general | solution.py:59
  173.9 4.7 copy.34
  178.8 12.5 %reduce-scatter.5.cloned.1.call-done = bf16[16,32,2048]{2,1,0:T(8,128)(2,1)} async-done(((bf16[32,32,2048]{2,1,0:T(8,128)(2,1)}), bf16[16,32,2048]{2,1,0:T(8,128)(2,1)}) %reduce-scatter.5.cloned.1.call-update) | async-done | bytes 2097168 | tf_op jit(solution)/shard_map/reduce_scatter | solution.py:18
  191.4 76.0 %reduce-scatter.7.cloned.1.call-done = bf16[1,32,2048]{2,1,0:T(8,128)(2,1)} async-done(((bf16[16,32,2048]{2,1,0:T(8,128)(2,1)}), bf16[1,32,2048]{2,1,0:T(8,128)(2,1)}) %reduce-scatter.7.cloned.1.call-update) | async-done | bytes 131088 | tf_op jit(solution)/shard_map/reduce_scatter | solution.py:18
  269.7 1.7 multiply_convert_fusion.3
  271.7 13.2 %all-gather.1 = bf16[256,1408]{1,0:T(8,128)(2,1)S(1)} all-gather(bf16[64,1408]{1,0:T(8,128)(2,1)S(1)} %get-tuple-element.21), channel_id=3, replica_groups=mesh['grp'=2,'fs_0'=16,'fs_1'=2,'tp'=4] {'tp'}, dimensions={0}, use_global_device_ids=true | all-gather | bytes 901120 | tf_op jit(solution)/shard_map/all_gather | solution.py:47
  286.4 2.7 all_to_all.64
  290.7 9.8 %all-to-all-start.2 = ((bf16[64,32,176]{2,0,1:T(8,128)(2,1)}), bf16[64,32,176]{2,0,1:T(8,128)(2,1)S(1)}, u32[]{:S(2)}, u32[]{:S(2)}) async-start(bf16[64,32,176]{2,0,1:T(8,128)(2,1)} %copy.36), calls=%async_computation.4 | async-start | bytes 2097152 | tf_op jit(solution)/shard_map/all_to_all | solution.py:52
  300.5 14.4 %all_gather.34 = bf16[64,5632]{1,0:T(8,128)(2,1)} all-gather(bf16[64,1408]{1,0:T(8,128)(2,1)S(1)} %get-tuple-element.22), channel_id=1, replica_groups=mesh['grp'=2,'fs_0'=16,'fs_1'=2,'tp'=4] {'tp'}, dimensions={1}, use_global_device_ids=true | all-gather | bytes 901120 | tf_op jit(solution)/shard_map/all_gather | solution.py:48
  314.9 3.8 all_to_all.68
  318.7 2.8 copy.37
  321.5 44.4 %all-to-all-done.2 = bf16[64,32,176]{2,0,1:T(8,128)(2,1)S(1)} async-done(((bf16[64,32,176]{2,0,1:T(8,128)(2,1)}), bf16[64,32,176]{2,0,1:T(8,128)(2,1)S(1)}, u32[]{:S(2)}, u32[]{:S(2)}) %all-to-all-start.2) | async-done | bytes 720928 | tf_op jit(solution)/shard_map/all_to_all | solution.py:52
  365.9 5.7 %all-to-all-start.3 = ((bf16[64,32,176]{2,0,1:T(8,128)(2,1)}), bf16[64,32,176]{2,0,1:T(8,128)(2,1)}, u32[]{:S(2)}, u32[]{:S(2)}) async-start(bf16[64,32,176]{2,0,1:T(8,128)(2,1)} %copy.37), calls=%async_computation.5 | async-start | bytes 2097152 | tf_op jit(solution)/shard_map/all_to_all | solution.py:53
  371.7 14.2 %all_gather.35 = bf16[176,2048]{1,0:T(8,128)(2,1)} all-gather(bf16[176,512]{1,0:T(8,128)(2,1)S(1)} %convert_element_type.74), channel_id=1, replica_groups=mesh['grp'=2,'fs_0'=16,'fs_1'=2,'tp'=4] {'tp'}, dimensions={1}, use_global_device_ids=true | all-gather | bytes 901120 | tf_op jit(solution)/shard_map/all_gather | solution.py:49
  385.9 4.6 fusion.29
  390.5 36.9 %all-to-all-done.3 = bf16[64,32,176]{2,0,1:T(8,128)(2,1)} async-done(((bf16[64,32,176]{2,0,1:T(8,128)(2,1)}), bf16[64,32,176]{2,0,1:T(8,128)(2,1)}, u32[]{:S(2)}, u32[]{:S(2)}) %all-to-all-start.3) | async-done | bytes 720928 | tf_op jit(solution)/shard_map/all_to_all | solution.py:53
  427.4 7.7 %convolution_convert_fusion = bf16[1024,2048]{1,0:T(8,128)(2,1)} fusion(bf16[176,2048]{1,0:T(8,128)(2,1)} %all_gather.35, bf16[1024,2048]{1,0:T(8,128)(2,1)} %all-gather.4.cloned.1.call-done, bf16[2048,176]{1,0:T(8,128)(2,1)} %bitcast.16, f32[1024,176]{0,1:T(8,128)} %fusion.29), kind=kOutput, calls=%fused_computation.4 | convolution fusion | flops 1479573504 | bytes 10551296 | tf_op jit(solution)/shard_map/dot_general | solution.py:59
  435.1 4.7 copy.38
  439.9 11.9 %reduce-scatter.9.cloned.1.call-done = bf16[16,32,2048]{2,1,0:T(8,128)(2,1)} async-done(((bf16[32,32,2048]{2,1,0:T(8,128)(2,1)}), bf16[16,32,2048]{2,1,0:T(8,128)(2,1)}) %reduce-scatter.9.cloned.1.call-update) | async-done | bytes 2097168 | tf_op jit(solution)/shard_map/reduce_scatter | solution.py:18
  453.1 2.3 copy.42
  457.8 69.9 %reduce-scatter.11.cloned.1.call-done = bf16[1,32,2048]{2,1,0:T(8,128)(2,1)} async-done(((bf16[16,32,2048]{2,1,0:T(8,128)(2,1)}), bf16[1,32,2048]{2,1,0:T(8,128)(2,1)}) %reduce-scatter.11.cloned.1.call-update) | async-done | bytes 131088 | tf_op jit(solution)/shard_map/reduce_scatter | solution.py:18
  530.0 1.9 multiply_convert_fusion.2
  (54 shorter events, 18.5 us)
Async XLA Ops:
  8.2 42.9 %copy-start.3 = (f32[64,1408]{1,0:T(8,128)S(1)}, f32[64,1408]{1,0:T(8,128)}, u32[]{:S(2)}) copy-start(f32[64,1408]{1,0:T(8,128)} %param.10) | copy-start | bytes 1081348
  41.5 64.9 %all-to-all-start = ((bf16[64,32,176]{2,0,1:T(8,128)(2,1)}), bf16[64,32,176]{2,0,1:T(8,128)(2,1)S(1)}, u32[]{:S(2)}, u32[]{:S(2)}) async-start(bf16[64,32,176]{2,0,1:T(8,128)(2,1)} %copy.32), calls=%async_computation | async-start | bytes 2097152 | tf_op jit(solution)/shard_map/all_to_all | solution.py:52
  51.1 60.2 %copy-start.4 = (f32[176,512]{1,0:T(8,128)S(1)}, f32[176,512]{1,0:T(8,128)}, u32[]{:S(2)}) copy-start(f32[176,512]{1,0:T(8,128)} %param.11) | copy-start | bytes 1081348
  106.4 60.6 %all-to-all-start.1 = ((bf16[64,32,176]{2,0,1:T(8,128)(2,1)}), bf16[64,32,176]{2,0,1:T(8,128)(2,1)S(1)}, u32[]{:S(2)}, u32[]{:S(2)}) async-start(bf16[64,32,176]{2,0,1:T(8,128)(2,1)} %copy.33), calls=%async_computation.1 | async-start | bytes 2097152 | tf_op jit(solution)/shard_map/all_to_all | solution.py:53
  111.3 80.0 %reduce-scatter.5.cloned.1.call-start = ((), (), s32[]{:S(2)}) async-start(), calls=%async_computation.8 | async-start | bytes 6291456 | tf_op jit(solution)/shard_map/reduce_scatter | solution.py:18
  125.7 41.3 %copy-start = (bf16[176,2048]{1,0:T(8,128)(2,1)}, bf16[176,2048]{1,0:T(8,128)(2,1)S(1)}, u32[]{:S(2)}) copy-start(bf16[176,2048]{1,0:T(8,128)(2,1)S(1)} %all_gather.30) | copy-start | bytes 2162692
  178.7 92.9 %copy-start.8 = (f32[2048]{0:T(1024)S(1)}, f32[2048]{0:T(1024)}, u32[]{:S(2)}) copy-start(f32[2048]{0:T(1024)} %param.12) | copy-start | bytes 24580
  178.7 93.0 %copy-start.6 = (f32[64,1408]{1,0:T(8,128)S(1)}, f32[64,1408]{1,0:T(8,128)}, u32[]{:S(2)}) copy-start(f32[64,1408]{1,0:T(8,128)} %param.13) | copy-start | bytes 1081348
  178.7 93.0 %copy-start.7 = (f32[64,1408]{1,0:T(8,128)S(1)}, f32[64,1408]{1,0:T(8,128)}, u32[]{:S(2)}) copy-start(f32[64,1408]{1,0:T(8,128)} %param.14) | copy-start | bytes 1081348
  178.7 88.7 %reduce-scatter.7.cloned.1.call-start = ((), (), s32[]{:S(2)}) async-start(), calls=%async_computation.9 | async-start | bytes 2228224 | tf_op jit(solution)/shard_map/reduce_scatter | solution.py:18
  191.4 194.5 %all-gather.4.cloned.1.call-start = ((), (), s32[]{:S(2)}) async-start(), calls=%async_computation.10 | async-start | bytes 4325376 | tf_op jit(solution)/shard_map/all_gather | solution.py:87
  290.7 75.2 %all-to-all-start.2 = ((bf16[64,32,176]{2,0,1:T(8,128)(2,1)}), bf16[64,32,176]{2,0,1:T(8,128)(2,1)S(1)}, u32[]{:S(2)}, u32[]{:S(2)}) async-start(bf16[64,32,176]{2,0,1:T(8,128)(2,1)} %copy.36), calls=%async_computation.4 | async-start | bytes 2097152 | tf_op jit(solution)/shard_map/all_to_all | solution.py:52
  314.9 56.8 %copy-start.5 = (f32[176,512]{1,0:T(8,128)S(1)}, f32[176,512]{1,0:T(8,128)}, u32[]{:S(2)}) copy-start(f32[176,512]{1,0:T(8,128)} %param.15) | copy-start | bytes 1081348
  365.9 61.5 %all-to-all-start.3 = ((bf16[64,32,176]{2,0,1:T(8,128)(2,1)}), bf16[64,32,176]{2,0,1:T(8,128)(2,1)}, u32[]{:S(2)}, u32[]{:S(2)}) async-start(bf16[64,32,176]{2,0,1:T(8,128)(2,1)} %copy.37), calls=%async_computation.5 | async-start | bytes 2097152 | tf_op jit(solution)/shard_map/all_to_all | solution.py:53
  371.6 80.2 %reduce-scatter.9.cloned.1.call-start = ((), (), s32[]{:S(2)}) async-start(), calls=%async_computation.11 | async-start | bytes 6291456 | tf_op jit(solution)/shard_map/reduce_scatter | solution.py:18
  439.8 87.8 %reduce-scatter.11.cloned.1.call-start = ((), (), s32[]{:S(2)}) async-start(), calls=%async_computation.12 | async-start | bytes 2228224 | tf_op jit(solution)/shard_map/reduce_scatter | solution.py:18
  453.1 78.8 %copy-start.1 = (bf16[176,2048]{1,0:T(8,128)(2,1)S(1)}, bf16[176,2048]{1,0:T(8,128)(2,1)}, u32[]{:S(2)}) copy-start(bf16[176,2048]{1,0:T(8,128)(2,1)} %copy-done) | copy-start | bytes 2162692
  453.1 79.6 %copy-start.2 = (bf16[176,2048]{1,0:T(8,128)(2,1)S(1)}, bf16[176,2048]{1,0:T(8,128)(2,1)}, u32[]{:S(2)}) copy-start(bf16[176,2048]{1,0:T(8,128)(2,1)} %all_gather.35) | copy-start | bytes 2162692
Sparse Core Ops, SparseCore 0:
  178.8 12.3 reduce-scatter.4
  193.8 73.5 reduce-scatter.6
  271.7 98.3 all-gather.3
  440.0 11.7 reduce-scatter.8
  454.2 73.4 reduce-scatter.10
